TPU v7x, 32 devices: a whole 2x2x4 slice. The times are simulated.
32 devices in a mesh: sp: 8 (over z, x), dp: 4 (over y, core).
Axes of the slice: x: 2, y: 2, z: 4, core: 2. Of those that a mesh axis runs over, the one named last changes fastest.
Arguments:
- queries: bfloat16 [4, 1024, 2048], P('dp', 'sp'), may hold values from -6 to 6
- keys: bfloat16 [4, 1024, 2048], P('dp', 'sp'), may hold values from -6 to 6
- values: bfloat16 [4, 1024, 2048], P('dp', 'sp'), may hold values from -6 to 6
- gate_totals: float32 [4, 1024, 32], P('dp', 'sp'), may hold values from -1024 to 0, as said below
- w_out: bfloat16 [2048, 2048], P(None, 'dp'), may hold values from -1 to 1
Outputs:
- mixed: bfloat16 [4, 1024, 2048], P('dp', 'sp')
Inputs may be any that keep to these rules, and one draw needn't show every extreme that they name: `gate_totals`: never rising along a sequence.
All inputs are finite; a program needn't handle non-finite values.
Results may differ from a plain program's by a relative error of at most 0.0053.
Values may be sent and summed in bfloat16 or wider, within the bound.
A program may use at most 64 MiB of HBM per device.

v0:
```python
import jax
import jax.numpy as jnp
from jax import lax
from jax.sharding import PartitionSpec as P

HEAD_DIM = 64


def attend(queries, key_rows, value_rows, totals):
    length = queries.shape[0]
    block_rows = min(length, 512)
    pieces = []
    for begin_row in range(0, length, block_rows):
        end_row = begin_row + block_rows
        scaled = queries[begin_row:end_row] * jnp.bfloat16(HEAD_DIM ** (-0.5))
        scores = jnp.einsum(
            "qhd,khd->hqk", scaled, key_rows[:end_row], preferred_element_type=jnp.float32
        )
        causal = jnp.arange(end_row)[None, :] <= (begin_row + jnp.arange(block_rows))[:, None]
        scores = jnp.where(
            causal[None],
            scores
            + jnp.transpose(totals[begin_row:end_row])[:, :, None]
            - jnp.transpose(totals[:end_row])[:, None, :],
            -jnp.inf,
        )
        biggest = jnp.max(scores, axis=-1, keepdims=True)
        expo = jnp.exp(scores - biggest)
        summed = jnp.sum(expo, axis=-1)
        weights = expo.astype(jnp.bfloat16)
        output = jnp.einsum(
            "hqk,khd->qhd", weights, value_rows[:end_row], preferred_element_type=jnp.float32
        )
        output = output / jnp.transpose(summed)[:, :, None]
        pieces.append(output.astype(jnp.bfloat16))
    return jnp.concatenate(pieces, axis=0).reshape(length, -1)


def local(queries, keys, values, gate_totals, w_out):
    moved = (
        lax.all_to_all(queries, "sp", split_axis=2, concat_axis=1, tiled=True),
        lax.all_to_all(keys, "sp", split_axis=2, concat_axis=1, tiled=True),
        lax.all_to_all(values, "sp", split_axis=2, concat_axis=1, tiled=True),
    )
    totals = lax.all_to_all(gate_totals, "sp", split_axis=2, concat_axis=1, tiled=True)
    held, length = (moved[0].shape[0], moved[0].shape[1])
    query_heads, key_heads, value_heads = [
        part_array[0].reshape(length, -1, HEAD_DIM) for part_array in moved
    ]
    outputs = [attend(query_heads, key_heads, value_heads, totals[0])]
    attended = jnp.stack(outputs, axis=0)
    local_rows = lax.all_to_all(attended, "sp", split_axis=1, concat_axis=2, tiled=True)
    flat_rows = local_rows.reshape(-1, local_rows.shape[2])
    mixed = jnp.dot(
        flat_rows,
        lax.all_gather(w_out, "dp", axis=1, tiled=True),
        preferred_element_type=jnp.float32,
    )
    return mixed.astype(jnp.bfloat16).reshape(local_rows.shape[0], local_rows.shape[1], -1)


def solution(mesh):
    placed = (
        P("dp", "sp", None),
        P("dp", "sp", None),
        P("dp", "sp", None),
        P("dp", "sp", None),
        P(None, "dp"),
    )
    return jax.shard_map(
        local, mesh=mesh, in_specs=placed, out_specs=P("dp", "sp", None), check_vma=False
    )
```

profile of v0, /device:TPU:0, one launch (start us, length us, event | category | flops | bytes accessed | tf_op | source)
XLA Modules:
  0.0 138.5 jit_solution(7458643636415226542)
XLA Ops:
  6.5 0.7 all-gather.2.cloned.1.call-update
  7.3 7.3 %all-to-all-start.2 = ((f32[1,128,32]{1,0,2:T(1,128)}), f32[1,128,32]{1,0,2:T(1,128)S(1)}, u32[]{:S(2)}, u32[]{:S(2)}) async-start(f32[1,128,32]{1,0,2:T(1,128)} %bitcast.98), calls=%async_computation.2 | async-start | bytes 32768 | tf_op jit(solution)/shard_map/all_to_all | solution.py:45
  14.6 2.3 %copy.32 = bf16[1,128,2048]{1,0,2:T(2,128)(2,1)S(1)} copy(bf16[1,128,2048]{2,1,0:T(8,128)(2,1)} %param.6) | data formatting | bytes 1048576 | tf_op args[1]
  16.9 0.6 broadcast.36
  17.5 11.6 %reduce.2 = bf16[2048,128]{1,0:T(8,128)(2,1)S(1)} reduce(bf16[2048,1,128]{2,1,0:T(2,128)(2,1)S(1)} %bitcast.83, bf16[]{:T(256)} %broadcast.36), dimensions={1}, to_apply=%bitcast.66.reduce_sub_computation | reduce | bytes 1048578
  29.0 1.0 reshape.70
  30.0 6.0 %all-to-all-start.1 = ((bf16[8,2,16384]{2,1,0:T(2,128)(2,1)}), bf16[8,2,16384]{2,1,0:T(2,128)(2,1)S(1)}, u32[]{:S(2)}, u32[]{:S(2)}) async-start(bf16[8,2,16384]{2,1,0:T(2,128)(2,1)} %reshape.70), calls=%async_computation.1 | async-start | bytes 1048576 | tf_op jit(solution)/shard_map/all_to_all | solution.py:42
  36.0 0.8 copy.35
  36.8 11.5 %reduce = bf16[2048,128]{1,0:T(8,128)(2,1)S(1)} reduce(bf16[2048,1,128]{2,1,0:T(2,128)(2,1)S(1)} %bitcast.85, bf16[]{:T(256)} %broadcast.36), dimensions={1}, to_apply=%bitcast.62.reduce_sub_computation | reduce | bytes 1048578
  48.3 0.9 reshape.66
  49.2 0.8 all-to-all-done.1
  50.0 5.2 %all-to-all-start.3 = ((bf16[8,2,16384]{2,1,0:T(2,128)(2,1)}), bf16[8,2,16384]{2,1,0:T(2,128)(2,1)S(1)}, u32[]{:S(2)}, u32[]{:S(2)}) async-start(bf16[8,2,16384]{2,1,0:T(2,128)(2,1)} %reshape.66), calls=%async_computation.3 | async-start | bytes 1048576 | tf_op jit(solution)/shard_map/all_to_all | solution.py:43
  55.2 0.8 copy.30
  56.0 11.5 %reduce.1 = bf16[2048,128]{1,0:T(8,128)(2,1)S(1)} reduce(bf16[2048,1,128]{2,1,0:T(2,128)(2,1)S(1)} %bitcast.86, bf16[]{:T(256)} %broadcast.36), dimensions={1}, to_apply=%bitcast.64.reduce_sub_computation | reduce | bytes 1048578
  67.5 1.0 reshape.68
  68.5 0.1 all-to-all-done.3
  68.6 5.9 %all-to-all-start = ((bf16[8,2,16384]{2,1,0:T(2,128)(2,1)}), bf16[8,2,16384]{2,1,0:T(2,128)(2,1)S(1)}, u32[]{:S(2)}, u32[]{:S(2)}) async-start(bf16[8,2,16384]{2,1,0:T(2,128)(2,1)} %reshape.68), calls=%async_computation | async-start | bytes 1048576 | tf_op jit(solution)/shard_map/all_to_all | solution.py:41
  74.5 0.4 iota_compare_fusion
  74.9 0.5 reshape.71
  75.5 0.3 copy.39
  75.9 0.7 slice.45
  76.6 0.5 reshape.67
  77.2 0.3 copy.40
  77.6 0.7 slice.43
  78.3 8.9 %all-to-all-done = bf16[8,2,16384]{2,1,0:T(2,128)(2,1)S(1)} async-done(((bf16[8,2,16384]{2,1,0:T(2,128)(2,1)}), bf16[8,2,16384]{2,1,0:T(2,128)(2,1)S(1)}, u32[]{:S(2)}, u32[]{:S(2)}) %all-to-all-start) | async-done | bytes 524320 | tf_op jit(solution)/shard_map/all_to_all | solution.py:41
  87.2 0.5 reshape.69
  87.9 0.2 copy.38
  88.1 0.8 mul.15
  89.0 1.0 reshape_squeeze.7
  90.0 0.2 reshape_squeeze.8
  90.2 0.2 copy.31
  90.4 0.1 mul.13
  90.5 0.2 copy.33
  90.7 0.1 slice.35
  90.9 0.2 copy.36
  91.2 1.2 fusion.8
  92.3 1.2 fusion.6
  93.6 1.4 %fusion.22 = bf16[512,4,64]{0,2,1:T(8,128)(2,1)S(1)} fusion(bf16[512,4,64]{0,2,1:T(8,128)(2,1)S(1)} %slice.39, f32[4,512,512]{1,2,0:T(8,128)S(1)} %get-tuple-element.12, f32[4,512]{1,0:T(4,128)S(1)} %get-tuple-element.11, f32[4,512]{1,0:T(4,128)S(1)} %get-tuple-element.7, pred[512,512]{0,1:T(8,128)(4,1)S(1)} %iota_compare_fusion.1, f32[512,4]{0,1:T(4,128)S(1)} %bitcast.100), kind=kOutput, calls=%fused_computation.21 | convolution fusion | flops 139722752 | bytes 5005312 | tf_op jit(solution)/shard_map/hqk,khd->qhd/dot_general | solution.py:31
  95.1 2.2 %fusion.2 = (f32[4,512]{1,0:T(4,128)S(1)}, f32[4,512,1024]{2,1,0:T(8,128)S(1)}) fusion(f32[4,1024]{1,0:T(4,128)S(1)} %bitcast.95, f32[4,512]{1,0:T(4,128)S(1)} %get-tuple-element.8, pred[512,1024]{1,0:T(8,128)(4,1)S(1)} %iota_compare_fusion, bf16[512,4,64]{0,2,1:T(8,128)(2,1)S(1)} %copy-done.5, bf16[1024,4,64]{0,2,1:T(8,128)(2,1)S(1)} %copy-done.4), kind=kOutput, calls=%fused_computation.4 | convolution fusion | flops 276822016 | bytes 9732096 | tf_op jit(solution)/shard_map/qhd,khd->hqk/dot_general | solution.py:16
  97.3 2.8 %fusion = f32[4,512]{1,0:T(4,128)S(1)} fusion(f32[4,512,1024]{2,1,0:T(8,128)S(1)} %get-tuple-element.10, f32[4,512]{1,0:T(4,128)S(1)} %get-tuple-element.9, f32[4,1024]{1,0:T(4,128)S(1)} %bitcast.96, f32[4,512]{1,0:T(4,128)S(1)} %get-tuple-element.8, pred[512,1024]{1,0:T(8,128)(4,1)S(1)} %iota_compare_fusion), kind=kLoop, calls=%fused_computation.2 | loop fusion | flops 10483712 | bytes 8953856 | tf_op jit(solution)/shard_map/reduce_sum | solution.py:29
  100.1 2.8 %fusion.28 = bf16[512,4,64]{0,2,1:T(8,128)(2,1)S(1)} fusion(bf16[1024,4,64]{0,2,1:T(8,128)(2,1)S(1)} %reshape_squeeze.8, f32[4,512,1024]{2,1,0:T(8,128)S(1)} %get-tuple-element.10, f32[4,512]{1,0:T(4,128)S(1)} %get-tuple-element.9, f32[4,1024]{1,0:T(4,128)S(1)} %bitcast.97, f32[4,512]{1,0:T(4,128)S(1)} %get-tuple-element.8, ...), kind=kOutput, calls=%fused_computation.23 | convolution fusion | flops 279183360 | bytes 9740288 | tf_op jit(solution)/shard_map/hqk,khd->qhd/dot_general | solution.py:31
  103.0 1.1 copy.41
  104.1 3.8 %reduce.3 = bf16[1024,256]{1,0:T(8,128)(2,1)S(1)} reduce(bf16[1024,1,256]{2,1,0:T(2,128)(2,1)S(1)} %bitcast.84, bf16[]{:T(256)} %broadcast.36), dimensions={1}, to_apply=%bitcast.68.reduce_sub_computation | reduce | bytes 1048578
  107.9 0.1 reshape.72
  108.0 17.2 %all_to_all.75 = bf16[8,2,16384]{2,1,0:T(2,128)(2,1)S(1)} all-to-all(bf16[8,2,16384]{2,1,0:T(2,128)(2,1)S(1)} %reshape.72), channel_id=1, replica_groups=mesh['sp'=8,'dp'=4] {'sp'}, dimensions={0} | all-to-all | bytes 1048576 | tf_op jit(solution)/shard_map/all_to_all | solution.py:52
  125.2 0.5 reshape.73
  125.9 0.3 copy.42
  126.2 5.5 %fusion.9 = bf16[1,128,2048]{2,1,0:T(8,128)(2,1)} fusion(bf16[128,2048]{0,1:T(8,128)(2,1)S(1)} %bitcast.78, bf16[2048,2048]{1,0:T(8,128)(2,1)} %all-gather.2.cloned.1.call-done), kind=kOutput, calls=%fused_computation.13 | convolution fusion | flops 1074003968 | bytes 9437184 | tf_op jit(solution)/shard_map/dot_general | solution.py:54
  (25 shorter events, 0.6 us)
Async XLA Ops:
  6.5 29.5 %copy-start.2 = (bf16[1,128,2048]{2,1,0:T(8,128)(2,1)S(1)}, bf16[1,128,2048]{2,1,0:T(8,128)(2,1)}, u32[]{:S(2)}) copy-start(bf16[1,128,2048]{2,1,0:T(8,128)(2,1)} %param.7) | copy-start | bytes 1572868
  6.5 119.6 %all-gather.2.cloned.1.call-start = ((), (), s32[]{:S(2)}) async-start(), calls=%async_computation.5 | async-start | bytes 10485760 | tf_op jit(solution)/shard_map/all_gather | solution.py:56
  7.3 22.8 %all-to-all-start.2 = ((f32[1,128,32]{1,0,2:T(1,128)}), f32[1,128,32]{1,0,2:T(1,128)S(1)}, u32[]{:S(2)}, u32[]{:S(2)}) async-start(f32[1,128,32]{1,0,2:T(1,128)} %bitcast.98), calls=%async_computation.2 | async-start | bytes 32768 | tf_op jit(solution)/shard_map/all_to_all | solution.py:45
  17.5 37.7 %copy-start.3 = (bf16[1,128,2048]{2,1,0:T(8,128)(2,1)S(1)}, bf16[1,128,2048]{2,1,0:T(8,128)(2,1)}, u32[]{:S(2)}) copy-start(bf16[1,128,2048]{2,1,0:T(8,128)(2,1)} %param.5) | copy-start | bytes 1572868
  30.0 20.0 %all-to-all-start.1 = ((bf16[8,2,16384]{2,1,0:T(2,128)(2,1)}), bf16[8,2,16384]{2,1,0:T(2,128)(2,1)S(1)}, u32[]{:S(2)}, u32[]{:S(2)}) async-start(bf16[8,2,16384]{2,1,0:T(2,128)(2,1)} %reshape.70), calls=%async_computation.1 | async-start | bytes 1048576 | tf_op jit(solution)/shard_map/all_to_all | solution.py:42
  50.0 18.6 %all-to-all-start.3 = ((bf16[8,2,16384]{2,1,0:T(2,128)(2,1)}), bf16[8,2,16384]{2,1,0:T(2,128)(2,1)S(1)}, u32[]{:S(2)}, u32[]{:S(2)}) async-start(bf16[8,2,16384]{2,1,0:T(2,128)(2,1)} %reshape.66), calls=%async_computation.3 | async-start | bytes 1048576 | tf_op jit(solution)/shard_map/all_to_all | solution.py:43
  68.6 18.7 %all-to-all-start = ((bf16[8,2,16384]{2,1,0:T(2,128)(2,1)}), bf16[8,2,16384]{2,1,0:T(2,128)(2,1)S(1)}, u32[]{:S(2)}, u32[]{:S(2)}) async-start(bf16[8,2,16384]{2,1,0:T(2,128)(2,1)} %reshape.68), calls=%async_computation | async-start | bytes 1048576 | tf_op jit(solution)/shard_map/all_to_all | solution.py:41
  87.8 2.7 %copy-start = (bf16[1,4,128,256]{2,3,1,0:T(8,128)(2,1)S(1)}, bf16[1,4,128,256]{2,3,1,0:T(8,128)(2,1)}, u32[]{:S(2)}) copy-start(bf16[1,4,128,256]{2,3,1,0:T(8,128)(2,1)} %slice.45) | copy-start | bytes 786436
  87.8 3.1 %copy-start.1 = (bf16[1,4,128,256]{2,3,1,0:T(8,128)(2,1)S(1)}, bf16[1,4,128,256]{2,3,1,0:T(8,128)(2,1)}, u32[]{:S(2)}) copy-start(bf16[1,4,128,256]{2,3,1,0:T(8,128)(2,1)} %slice.43) | copy-start | bytes 786436
  93.6 1.5 %copy-start.4 = (bf16[1024,4,64]{0,2,1:T(8,128)(2,1)S(1)}, bf16[1024,4,64]{0,2,1:T(8,128)(2,1)}, u32[]{:S(2)}) copy-start(bf16[1024,4,64]{0,2,1:T(8,128)(2,1)} %reshape_squeeze.7) | copy-start | bytes 1572868
  93.6 1.5 %copy-start.5 = (bf16[512,4,64]{0,2,1:T(8,128)(2,1)S(1)}, bf16[512,4,64]{0,2,1:T(8,128)(2,1)}, u32[]{:S(2)}) copy-start(bf16[512,4,64]{0,2,1:T(8,128)(2,1)} %mul.15) | copy-start | bytes 786436
Sparse Core Ops, SparseCore 0:
  8.9 60.9 all-gather.1
where the time goes:
time: 139 us; the launch traced here: 138 us
  other arithmetic  43 us (31%)
  starting transfers between devices  24.4 us (18%)
  blocking collectives  17.2 us (12%)
  local copies, waits for them, and re-layouts  16.5 us (12%)
  between operations  13.7 us (10%)
  matrix products  13.1 us (9%)
  waiting for transfers between devices  10.5 us (8%)
    unnamed x4, other arithmetic  38.4 us
    all_to_all x1, blocking collectives, local(): lax.all_to_all(attended, 'sp', split_axis=1, concat_axis=2, tiled=True)  17.2 us
    unnamed x28, local copies, waits for them, and re-layouts  9.83 us
    all_to_all x1, waiting for transfers between devices, local(): lax.all_to_all(queries, 'sp', split_axis=2, concat_axis=1, tiled=True)  8.91 us
    all_to_all x1, starting transfers between devices, local(): lax.all_to_all(gate_totals, 'sp', split_axis=2, concat_axis=1, tiled=True)  7.29 us
    all_to_all x1, starting transfers between devices, local(): lax.all_to_all(keys, 'sp', split_axis=2, concat_axis=1, tiled=True)  6 us
    all_to_all x1, starting transfers between devices, local(): lax.all_to_all(queries, 'sp', split_axis=2, concat_axis=1, tiled=True)  5.88 us
    dot_general x1, matrix products, local(): jnp.dot(flat_rows, lax.all_gather(w_out, 'dp', axis=1, tiled=True), prefe...  5.46 us
  transfers between devices with their start and end apart: 5, of which 3 were waited for; matrix products, arithmetic and copies ran while one was open for 48% of the time, Pallas kernels for 0%

commit v1 on v0

--- a/solution.py
+++ b/solution.py
@@ -38,7 +38,10 @@
 
 def local(queries, keys, values, gate_totals, w_out):
     moved = (
-        lax.all_to_all(queries, "sp", split_axis=2, concat_axis=1, tiled=True),
+        jnp.concatenate(
+            lax.all_to_all(jnp.stack(jnp.split(queries, lax.axis_size("sp"), axis=2)), "sp", 0, 0),
+            axis=1,
+        ),
         lax.all_to_all(keys, "sp", split_axis=2, concat_axis=1, tiled=True),
         lax.all_to_all(values, "sp", split_axis=2, concat_axis=1, tiled=True),
     )

time: 139 us -> 138 us (level)
  other arithmetic: 43 us -> 31.4 us
  waiting for transfers between devices: 10.5 us -> 20.6 us
  local copies, waits for them, and re-layouts: 16.5 us -> 18.4 us
  starting transfers between devices: 24.4 us -> 23 us
    unnamed x4 -> x3, other arithmetic: 38.4 us -> 26.8 us
    all_to_all x1, waiting for transfers between devices: 0.11 us -> 10.2 us  [local(): lax.all_to_all(values, 'sp', split_axis=2, concat_axis=1, tiled=True)]
    all_to_all x1, starting transfers between devices: 5.88 us -> 3.68 us  [local(): lax.all_to_all(jnp.stack(jnp.split(queries, lax.axis_size('sp'), axis=2))...]
    unnamed x28 -> x29, local copies, waits for them, and re-layouts: 9.83 us -> 11.9 us
  transfers between devices with their start and end apart: 5 -> 5, of which waited for: 3 -> 2; matrix products, arithmetic and copies ran while one was open for 48% -> 42% of each run, Pallas kernels for 0% -> 0%
where the time goes in v1:
time: 138 us
  other arithmetic  31.4 us (23%)
  starting transfers between devices  23 us (17%)
  waiting for transfers between devices  20.6 us (15%)
  local copies, waits for them, and re-layouts  18.4 us (13%)
  blocking collectives  17.5 us (13%)
  between operations  13.7 us (10%)
  matrix products  13.1 us (9%)
    unnamed x3, other arithmetic  26.8 us
    all_to_all x1, blocking collectives, local(): lax.all_to_all(attended, 'sp', split_axis=1, concat_axis=2, tiled=True)  17.5 us
    unnamed x29, local copies, waits for them, and re-layouts  11.9 us
    all_to_all x1, waiting for transfers between devices, local(): lax.all_to_all(values, 'sp', split_axis=2, concat_axis=1, tiled=True)  10.2 us
    all_to_all x1, waiting for transfers between devices, local(): lax.all_to_all(jnp.stack(jnp.split(queries, lax.axis_size('sp'), axis=2))...  9.62 us
    all_to_all x1, starting transfers between devices, local(): lax.all_to_all(gate_totals, 'sp', split_axis=2, concat_axis=1, tiled=True)  7.29 us
    all_to_all x1, starting transfers between devices, local(): lax.all_to_all(keys, 'sp', split_axis=2, concat_axis=1, tiled=True)  6 us
    all_to_all x1, starting transfers between devices, local(): lax.all_to_all(values, 'sp', split_axis=2, concat_axis=1, tiled=True)  5.99 us
  transfers between devices with their start and end apart: 5, of which 2 were waited for; matrix products, arithmetic and copies ran while one was open for 42% of the time, Pallas kernels for 0%

profile of v1, /device:TPU:0, one launch (start us, length us, event | category | flops | bytes accessed | tf_op | source)
XLA Modules:
  0.0 137.8 jit_solution(782201972838408311)
XLA Ops:
  6.5 0.7 all-gather.2.cloned.1.call-update
  7.3 7.3 %all-to-all-start.2 = ((f32[1,128,32]{1,0,2:T(1,128)}), f32[1,128,32]{1,0,2:T(1,128)S(1)}, u32[]{:S(2)}, u32[]{:S(2)}) async-start(f32[1,128,32]{1,0,2:T(1,128)} %bitcast.106), calls=%async_computation.2 | async-start | bytes 32768 | tf_op jit(solution)/shard_map/all_to_all | solution.py:48
  14.6 2.3 %copy.34 = bf16[1,128,2048]{1,0,2:T(2,128)(2,1)S(1)} copy(bf16[1,128,2048]{2,1,0:T(8,128)(2,1)} %param.6) | data formatting | bytes 1048576 | tf_op args[1]
  16.9 0.6 broadcast.36
  17.5 11.5 %reduce.1 = bf16[2048,128]{1,0:T(8,128)(2,1)S(1)} reduce(bf16[2048,1,128]{2,1,0:T(2,128)(2,1)S(1)} %bitcast.93, bf16[]{:T(256)} %broadcast.36), dimensions={1}, to_apply=%bitcast.77.reduce_sub_computation | reduce | bytes 1048578
  29.0 1.0 reshape.67
  30.0 6.0 %all-to-all-start.1 = ((bf16[8,2,16384]{2,1,0:T(2,128)(2,1)}), bf16[8,2,16384]{2,1,0:T(2,128)(2,1)S(1)}, u32[]{:S(2)}, u32[]{:S(2)}) async-start(bf16[8,2,16384]{2,1,0:T(2,128)(2,1)} %reshape.67), calls=%async_computation.1 | async-start | bytes 1048576 | tf_op jit(solution)/shard_map/all_to_all | solution.py:45
  36.0 0.8 copy.37
  36.7 11.5 %reduce = bf16[2048,128]{1,0:T(8,128)(2,1)S(1)} reduce(bf16[2048,1,128]{2,1,0:T(2,128)(2,1)S(1)} %bitcast.95, bf16[]{:T(256)} %broadcast.36), dimensions={1}, to_apply=%bitcast.75.reduce_sub_computation | reduce | bytes 1048578
  48.2 0.9 reshape.65
  49.2 0.6 bitcast_dynamic-update-slice_fusion.7
  49.8 0.6 bitcast_dynamic-update-slice_fusion.6
  50.4 0.6 bitcast_dynamic-update-slice_fusion.5
  51.0 6.0 %all-to-all-start.3 = ((bf16[8,2,16384]{2,1,0:T(2,128)(2,1)}), bf16[8,2,16384]{2,1,0:T(2,128)(2,1)S(1)}, u32[]{:S(2)}, u32[]{:S(2)}) async-start(bf16[8,2,16384]{2,1,0:T(2,128)(2,1)} %reshape.65), calls=%async_computation.3 | async-start | bytes 1048576 | tf_op jit(solution)/shard_map/all_to_all | solution.py:46
  57.0 0.6 bitcast_dynamic-update-slice_fusion.4
  57.7 0.6 bitcast_dynamic-update-slice_fusion.3
  58.3 0.6 bitcast_dynamic-update-slice_fusion.2
  58.9 0.6 bitcast_dynamic-update-slice_fusion.1
  59.5 0.6 bitcast_dynamic-update-slice_fusion
  60.2 10.2 %all-to-all-done.3 = bf16[8,2,16384]{2,1,0:T(2,128)(2,1)S(1)} async-done(((bf16[8,2,16384]{2,1,0:T(2,128)(2,1)}), bf16[8,2,16384]{2,1,0:T(2,128)(2,1)S(1)}, u32[]{:S(2)}, u32[]{:S(2)}) %all-to-all-start.3) | async-done | bytes 524320 | tf_op jit(solution)/shard_map/all_to_all | solution.py:46
  70.4 3.7 %all-to-all-start = ((bf16[8,1,128,256]{3,2,1,0:T(8,128)(2,1)}), bf16[8,1,128,256]{3,2,1,0:T(8,128)(2,1)S(1)}, u32[]{:S(2)}, u32[]{:S(2)}) async-start(bf16[8,1,128,256]{3,2,1,0:T(8,128)(2,1)} %bitcast_dynamic-update-slice_fusion), calls=%async_computation | async-start | bytes 1048576 | tf_op jit(solution)/shard_map/all_to_all | solution.py:42
  74.2 0.4 iota_compare_fusion
  74.6 0.5 reshape.68
  75.2 0.3 copy.41
  75.5 0.7 slice.45
  76.3 0.5 reshape.66
  76.9 0.3 copy.42
  77.3 1.0 reshape_squeeze.6
  78.3 9.6 %all-to-all-done = bf16[8,1,128,256]{3,2,1,0:T(8,128)(2,1)S(1)} async-done(((bf16[8,1,128,256]{3,2,1,0:T(8,128)(2,1)}), bf16[8,1,128,256]{3,2,1,0:T(8,128)(2,1)S(1)}, u32[]{:S(2)}, u32[]{:S(2)}) %all-to-all-start) | async-done | bytes 524320 | tf_op jit(solution)/shard_map/all_to_all | solution.py:42
  87.9 0.2 copy.40
  88.1 0.8 mul.15
  88.9 0.2 reshape_squeeze.7
  89.2 0.2 copy.35
  89.5 0.2 copy.33
  89.8 0.2 copy.38
  90.1 1.2 fusion.8
  91.3 1.2 fusion.6
  92.6 1.4 %fusion.22 = bf16[512,4,64]{0,2,1:T(8,128)(2,1)S(1)} fusion(bf16[512,4,64]{0,2,1:T(8,128)(2,1)S(1)} %slice.39, f32[4,512,512]{1,2,0:T(8,128)S(1)} %get-tuple-element.12, f32[4,512]{1,0:T(4,128)S(1)} %get-tuple-element.11, f32[4,512]{1,0:T(4,128)S(1)} %get-tuple-element.7, pred[512,512]{0,1:T(8,128)(4,1)S(1)} %iota_compare_fusion.1, f32[512,4]{0,1:T(4,128)S(1)} %bitcast.108), kind=kOutput, calls=%fused_computation.21 | convolution fusion | flops 139722752 | bytes 5005312 | tf_op jit(solution)/shard_map/hqk,khd->qhd/dot_general | solution.py:31
  94.0 2.3 %fusion.2 = (f32[4,512]{1,0:T(4,128)S(1)}, f32[4,512,1024]{2,1,0:T(8,128)S(1)}) fusion(f32[4,1024]{1,0:T(4,128)S(1)} %bitcast.103, f32[4,512]{1,0:T(4,128)S(1)} %get-tuple-element.8, pred[512,1024]{1,0:T(8,128)(4,1)S(1)} %iota_compare_fusion, bf16[512,4,64]{0,2,1:T(8,128)(2,1)S(1)} %copy-done.4, bf16[1024,4,64]{0,2,1:T(8,128)(2,1)S(1)} %copy-done.3), kind=kOutput, calls=%fused_computation.4 | convolution fusion | flops 276822016 | bytes 9732096 | tf_op jit(solution)/shard_map/qhd,khd->hqk/dot_general | solution.py:16
  96.3 2.8 %fusion = f32[4,512]{1,0:T(4,128)S(1)} fusion(f32[4,512,1024]{2,1,0:T(8,128)S(1)} %get-tuple-element.10, f32[4,512]{1,0:T(4,128)S(1)} %get-tuple-element.9, f32[4,1024]{1,0:T(4,128)S(1)} %bitcast.104, f32[4,512]{1,0:T(4,128)S(1)} %get-tuple-element.8, pred[512,1024]{1,0:T(8,128)(4,1)S(1)} %iota_compare_fusion), kind=kLoop, calls=%fused_computation.2 | loop fusion | flops 10483712 | bytes 8953856 | tf_op jit(solution)/shard_map/reduce_sum | solution.py:29
  99.1 2.8 %fusion.28 = bf16[512,4,64]{0,2,1:T(8,128)(2,1)S(1)} fusion(bf16[1024,4,64]{0,2,1:T(8,128)(2,1)S(1)} %reshape_squeeze.7, f32[4,512,1024]{2,1,0:T(8,128)S(1)} %get-tuple-element.10, f32[4,512]{1,0:T(4,128)S(1)} %get-tuple-element.9, f32[4,1024]{1,0:T(4,128)S(1)} %bitcast.105, f32[4,512]{1,0:T(4,128)S(1)} %get-tuple-element.8, ...), kind=kOutput, calls=%fused_computation.23 | convolution fusion | flops 279183360 | bytes 9740288 | tf_op jit(solution)/shard_map/hqk,khd->qhd/dot_general | solution.py:31
  102.0 1.1 copy.43
  103.0 3.8 %reduce.2 = bf16[1024,256]{1,0:T(8,128)(2,1)S(1)} reduce(bf16[1024,1,256]{2,1,0:T(2,128)(2,1)S(1)} %bitcast.94, bf16[]{:T(256)} %broadcast.36), dimensions={1}, to_apply=%bitcast.79.reduce_sub_computation | reduce | bytes 1048578
  106.9 0.1 reshape.69
  107.0 17.5 %all_to_all.65 = bf16[8,2,16384]{2,1,0:T(2,128)(2,1)S(1)} all-to-all(bf16[8,2,16384]{2,1,0:T(2,128)(2,1)S(1)} %reshape.69), channel_id=1, replica_groups=mesh['sp'=8,'dp'=4] {'sp'}, dimensions={0} | all-to-all | bytes 1048576 | tf_op jit(solution)/shard_map/all_to_all | solution.py:55
  124.5 0.5 reshape.70
  125.2 0.3 copy.44
  125.5 5.5 %fusion.9 = bf16[1,128,2048]{2,1,0:T(8,128)(2,1)} fusion(bf16[128,2048]{0,1:T(8,128)(2,1)S(1)} %bitcast.89, bf16[2048,2048]{1,0:T(8,128)(2,1)} %all-gather.2.cloned.1.call-done), kind=kOutput, calls=%fused_computation.13 | convolution fusion | flops 1074003968 | bytes 9437184 | tf_op jit(solution)/shard_map/dot_general | solution.py:57
  (26 shorter events, 0.8 us)
Async XLA Ops:
  6.5 29.4 %copy-start.1 = (bf16[1,128,2048]{2,1,0:T(8,128)(2,1)S(1)}, bf16[1,128,2048]{2,1,0:T(8,128)(2,1)}, u32[]{:S(2)}) copy-start(bf16[1,128,2048]{2,1,0:T(8,128)(2,1)} %param.7) | copy-start | bytes 1572868
  6.5 118.9 %all-gather.2.cloned.1.call-start = ((), (), s32[]{:S(2)}) async-start(), calls=%async_computation.5 | async-start | bytes 10485760 | tf_op jit(solution)/shard_map/all_gather | solution.py:59
  7.3 22.7 %all-to-all-start.2 = ((f32[1,128,32]{1,0,2:T(1,128)}), f32[1,128,32]{1,0,2:T(1,128)S(1)}, u32[]{:S(2)}, u32[]{:S(2)}) async-start(f32[1,128,32]{1,0,2:T(1,128)} %bitcast.106), calls=%async_computation.2 | async-start | bytes 32768 | tf_op jit(solution)/shard_map/all_to_all | solution.py:48
  16.9 32.3 %copy-start.2 = (bf16[1,128,2048]{2,1,0:T(8,128)(2,1)S(1)}, bf16[1,128,2048]{2,1,0:T(8,128)(2,1)}, u32[]{:S(2)}) copy-start(bf16[1,128,2048]{2,1,0:T(8,128)(2,1)} %param.5) | copy-start | bytes 1572868
  30.0 21.1 %all-to-all-start.1 = ((bf16[8,2,16384]{2,1,0:T(2,128)(2,1)}), bf16[8,2,16384]{2,1,0:T(2,128)(2,1)S(1)}, u32[]{:S(2)}, u32[]{:S(2)}) async-start(bf16[8,2,16384]{2,1,0:T(2,128)(2,1)} %reshape.67), calls=%async_computation.1 | async-start | bytes 1048576 | tf_op jit(solution)/shard_map/all_to_all | solution.py:45
  51.0 19.4 %all-to-all-start.3 = ((bf16[8,2,16384]{2,1,0:T(2,128)(2,1)}), bf16[8,2,16384]{2,1,0:T(2,128)(2,1)S(1)}, u32[]{:S(2)}, u32[]{:S(2)}) async-start(bf16[8,2,16384]{2,1,0:T(2,128)(2,1)} %reshape.65), calls=%async_computation.3 | async-start | bytes 1048576 | tf_op jit(solution)/shard_map/all_to_all | solution.py:46
  70.4 17.5 %all-to-all-start = ((bf16[8,1,128,256]{3,2,1,0:T(8,128)(2,1)}), bf16[8,1,128,256]{3,2,1,0:T(8,128)(2,1)S(1)}, u32[]{:S(2)}, u32[]{:S(2)}) async-start(bf16[8,1,128,256]{3,2,1,0:T(8,128)(2,1)} %bitcast_dynamic-update-slice_fusion), calls=%async_computation | async-start | bytes 1048576 | tf_op jit(solution)/shard_map/all_to_all | solution.py:42
  76.8 12.4 %copy-start = (bf16[1,4,128,256]{2,3,1,0:T(8,128)(2,1)S(1)}, bf16[1,4,128,256]{2,3,1,0:T(8,128)(2,1)}, u32[]{:S(2)}) copy-start(bf16[1,4,128,256]{2,3,1,0:T(8,128)(2,1)} %slice.45) | copy-start | bytes 786436
  92.5 1.5 %copy-start.3 = (bf16[1024,4,64]{0,2,1:T(8,128)(2,1)S(1)}, bf16[1024,4,64]{0,2,1:T(8,128)(2,1)}, u32[]{:S(2)}) copy-start(bf16[1024,4,64]{0,2,1:T(8,128)(2,1)} %reshape_squeeze.6) | copy-start | bytes 1572868
  92.5 1.5 %copy-start.4 = (bf16[512,4,64]{0,2,1:T(8,128)(2,1)S(1)}, bf16[512,4,64]{0,2,1:T(8,128)(2,1)}, u32[]{:S(2)}) copy-start(bf16[512,4,64]{0,2,1:T(8,128)(2,1)} %mul.15) | copy-start | bytes 786436
Sparse Core Ops, SparseCore 0:
  8.9 60.9 all-gather.1
